TPU v7x, 32 devices: a whole 2x2x4 slice. The times are simulated.
32 devices in a mesh: sp: 4 (over y, core), dp: 8 (over z, x).
Axes of the slice: x: 2, y: 2, z: 4, core: 2. Of those that a mesh axis runs over, the one named last changes fastest.
Arguments:
- queries: bfloat16 [8, 1024, 1024], P('dp', 'sp'), may hold values from -250 to 250
- keys: bfloat16 [8, 1024, 1024], P('dp', 'sp'), may hold values from -6 to 6
- values: bfloat16 [8, 1024, 1024], P('dp', 'sp'), may hold values from -6 to 6
- cum_gate: float32 [8, 16, 1024], P('dp', 'sp'), may hold values from -1024 to 0, as said below
- out_weight: bfloat16 [1024, 2112], P(None, 'dp'), may hold values from -1.5 to 1.5
Outputs:
- mixed: bfloat16 [8, 1024, 2112], P('dp', 'sp')
Inputs may be any that keep to these rules, and one draw needn't show every extreme that they name: `cum_gate`: within each head the entries do not rise along positions.
All inputs are finite; a program needn't handle non-finite values.
Results may differ from a plain program's by a relative error of at most 0.0053.
Values may be sent and summed in bfloat16 or wider, within the bound.
A program may use at most 64 MiB of HBM per device.

v0:
```python
import jax
import jax.numpy as jnp
from jax import lax
from jax.sharding import PartitionSpec as P


def attend(query_all, key_all, value_all, gate_all):
    length, width = query_all.shape
    heads = gate_all.shape[0]
    depth = width // heads
    block_rows = min(512, length)
    block_count = length // block_rows
    score_scale = depth ** (-0.5)
    query_blocks = query_all.reshape(block_count, block_rows, heads, depth)
    key_blocks = key_all.reshape(block_count, block_rows, heads, depth)
    value_blocks = value_all.reshape(block_count, block_rows, heads, depth)
    gate_blocks = gate_all.reshape(heads, block_count, block_rows).transpose(1, 0, 2)
    offsets = jnp.arange(block_rows, dtype=jnp.int32)

    def one_block(block_index):
        query_part = lax.dynamic_index_in_dim(query_blocks, block_index, 0, keepdims=False)
        gate_part = lax.dynamic_index_in_dim(gate_blocks, block_index, 0, keepdims=False)
        query_rows = block_index * block_rows + offsets

        def key_step(key_block, carry):
            running_max, running_sum, weighted = carry
            key_part = lax.dynamic_index_in_dim(key_blocks, key_block, 0, keepdims=False)
            value_part = lax.dynamic_index_in_dim(value_blocks, key_block, 0, keepdims=False)
            gate_keys = lax.dynamic_index_in_dim(gate_blocks, key_block, 0, keepdims=False)
            logits = (
                jnp.einsum("qhe,khe->hqk", query_part, key_part, preferred_element_type=jnp.float32)
                * score_scale
            )
            logits = logits + gate_part[:, :, None] - gate_keys[:, None, :]
            key_rows = key_block * block_rows + offsets
            allowed = key_rows[None, :] <= query_rows[:, None]
            logits = jnp.where(allowed[None], logits, -jnp.inf)
            new_max = jnp.maximum(running_max, jnp.max(logits, axis=-1))
            scores = jnp.exp(logits - new_max[..., None])
            factor = jnp.exp(running_max - new_max)
            running_sum = running_sum * factor + jnp.sum(scores, axis=-1)
            weighted = weighted * factor[..., None] + jnp.einsum(
                "hqk,khe->hqe",
                scores.astype(jnp.bfloat16),
                value_part,
                preferred_element_type=jnp.float32,
            )
            return (new_max, running_sum, weighted)

        start_state = (
            jnp.full((heads, block_rows), -jnp.inf, jnp.float32),
            jnp.zeros((heads, block_rows), jnp.float32),
            jnp.zeros((heads, block_rows, depth), jnp.float32),
        )
        final_max, final_sum, weighted = lax.fori_loop(0, block_index + 1, key_step, start_state)
        result = weighted / final_sum[..., None]
        return result.transpose(1, 0, 2).astype(jnp.bfloat16)

    outputs = lax.map(one_block, jnp.arange(block_count, dtype=jnp.int32))
    return outputs.reshape(length, width)


def body(queries, keys, values, cum_gate, out_weight):
    query_heads, key_heads, value_heads = (
        lax.all_to_all(queries, "sp", split_axis=2, concat_axis=1, tiled=True),
        lax.all_to_all(keys, "sp", split_axis=2, concat_axis=1, tiled=True),
        lax.all_to_all(values, "sp", split_axis=2, concat_axis=1, tiled=True),
    )
    local_out = attend(query_heads[0], key_heads[0], value_heads[0], cum_gate[0])
    attended = lax.all_to_all(local_out[None], "sp", split_axis=1, concat_axis=2, tiled=True)[0]
    group_rows = attended.shape[1] // lax.axis_size("sp")
    own_rows = lax.dynamic_slice_in_dim(
        out_weight, lax.axis_index("sp") * group_rows, group_rows, 0
    )
    full_rows = lax.all_gather(own_rows, "dp", axis=1, tiled=True)
    whole_weight = lax.all_gather(full_rows, "sp", axis=0, tiled=True)
    mixed = jnp.dot(attended, whole_weight, preferred_element_type=jnp.float32)
    return mixed.astype(jnp.bfloat16)[None]


def solution(mesh):
    in_specs = (
        P("dp", "sp", None),
        P("dp", "sp", None),
        P("dp", "sp", None),
        P("dp", "sp", None),
        P(None, "dp"),
    )
    out_specs = P("dp", "sp", None)
    return jax.shard_map(body, mesh=mesh, in_specs=in_specs, out_specs=out_specs, check_vma=False)
```

profile of v0, /device:TPU:0, one launch (start us, length us, event | category | flops | bytes accessed | tf_op | source)
XLA Modules:
  0.0 110.8 jit_solution(6020720090809697798)
XLA Ops:
  6.5 1.0 copy-done
  7.6 0.7 constant_dynamic-slice_fusion
  8.3 2.4 %copy.29 = bf16[1,256,1024]{1,0,2:T(2,128)(2,1)S(1)} copy(bf16[1,256,1024]{2,1,0:T(8,128)(2,1)} %param.9) | data formatting | bytes 1048576 | tf_op args[0]
  10.7 0.5 broadcast.54
  11.2 3.8 %reduce = bf16[1024,256]{1,0:T(8,128)(2,1)S(1)} reduce(bf16[1024,1,256]{2,1,0:T(2,128)(2,1)S(1)} %bitcast.91, bf16[]{:T(256)} %broadcast.54), dimensions={1}, to_apply=%bitcast.52.reduce_sub_computation | reduce | bytes 1048578
  15.0 0.9 reshape.40
  15.9 4.3 %all-to-all-start = ((bf16[4,2,32768]{2,1,0:T(2,128)(2,1)}), bf16[4,2,32768]{2,1,0:T(2,128)(2,1)S(1)}, u32[]{:S(2)}, u32[]{:S(2)}) async-start(bf16[4,2,32768]{2,1,0:T(2,128)(2,1)} %reshape.40), calls=%async_computation | async-start | bytes 1048576 | tf_op jit(solution)/shard_map/all_to_all | solution.py:65
  20.2 0.8 copy.31
  21.0 3.8 %reduce.1 = bf16[1024,256]{1,0:T(8,128)(2,1)S(1)} reduce(bf16[1024,1,256]{2,1,0:T(2,128)(2,1)S(1)} %bitcast.93, bf16[]{:T(256)} %broadcast.54), dimensions={1}, to_apply=%bitcast.54.reduce_sub_computation | reduce | bytes 1048578
  24.9 0.9 reshape.42
  25.8 3.2 %all-to-all-done = bf16[4,2,32768]{2,1,0:T(2,128)(2,1)S(1)} async-done(((bf16[4,2,32768]{2,1,0:T(2,128)(2,1)}), bf16[4,2,32768]{2,1,0:T(2,128)(2,1)S(1)}, u32[]{:S(2)}, u32[]{:S(2)}) %all-to-all-start) | async-done | bytes 524320 | tf_op jit(solution)/shard_map/all_to_all | solution.py:65
  29.0 3.5 %all-to-all-start.1 = ((bf16[4,2,32768]{2,1,0:T(2,128)(2,1)}), bf16[4,2,32768]{2,1,0:T(2,128)(2,1)S(1)}, u32[]{:S(2)}, u32[]{:S(2)}) async-start(bf16[4,2,32768]{2,1,0:T(2,128)(2,1)} %reshape.42), calls=%async_computation.1 | async-start | bytes 1048576 | tf_op jit(solution)/shard_map/all_to_all | solution.py:66
  32.5 2.4 %copy.33 = bf16[1,256,1024]{1,0,2:T(2,128)(2,1)S(1)} copy(bf16[1,256,1024]{2,1,0:T(8,128)(2,1)} %param.11) | data formatting | bytes 1048576 | tf_op args[2]
  34.9 3.8 %reduce.2 = bf16[1024,256]{1,0:T(8,128)(2,1)S(1)} reduce(bf16[1024,1,256]{2,1,0:T(2,128)(2,1)S(1)} %bitcast.94, bf16[]{:T(256)} %broadcast.54), dimensions={1}, to_apply=%bitcast.56.reduce_sub_computation | reduce | bytes 1048578
  38.7 0.9 reshape.44
  39.6 1.7 %all-to-all-done.1 = bf16[4,2,32768]{2,1,0:T(2,128)(2,1)S(1)} async-done(((bf16[4,2,32768]{2,1,0:T(2,128)(2,1)}), bf16[4,2,32768]{2,1,0:T(2,128)(2,1)S(1)}, u32[]{:S(2)}, u32[]{:S(2)}) %all-to-all-start.1) | async-done | bytes 524320 | tf_op jit(solution)/shard_map/all_to_all | solution.py:66
  41.3 4.1 %all-to-all-start.2 = ((bf16[4,2,32768]{2,1,0:T(2,128)(2,1)}), bf16[4,2,32768]{2,1,0:T(2,128)(2,1)}, u32[]{:S(2)}, u32[]{:S(2)}) async-start(bf16[4,2,32768]{2,1,0:T(2,128)(2,1)} %reshape.44), calls=%async_computation.2 | async-start | bytes 1048576 | tf_op jit(solution)/shard_map/all_to_all | solution.py:67
  45.4 0.2 all-gather.5.cloned.1.call-start
  45.6 0.5 reshape.41
  46.2 0.1 copy.44
  46.3 0.4 copy.30
  46.7 0.3 reshape_squeeze.12
  47.0 0.1 copy.35
  47.1 0.5 reshape.43
  47.6 0.1 copy.45
  47.7 0.4 copy.32
  48.2 0.3 reshape_squeeze.14
  48.5 0.1 copy.36
  48.6 5.7 %all-to-all-done.2 = bf16[4,2,32768]{2,1,0:T(2,128)(2,1)} async-done(((bf16[4,2,32768]{2,1,0:T(2,128)(2,1)}), bf16[4,2,32768]{2,1,0:T(2,128)(2,1)}, u32[]{:S(2)}, u32[]{:S(2)}) %all-to-all-start.2) | async-done | bytes 524320 | tf_op jit(solution)/shard_map/all_to_all | solution.py:67
  54.3 2.2 %reshape.45 = bf16[1024,1,256]{2,1,0:T(2,128)(2,1)S(1)} reshape(bf16[4,2,32768]{2,1,0:T(2,128)(2,1)} %all-to-all-done.2) | data formatting | bytes 1048576
  56.5 0.1 copy.46
  56.6 0.4 copy.34
  57.0 0.3 reshape_squeeze.15
  57.3 0.9 copy.37
  58.2 0.0 all-gather.5.cloned.1.call-update
  58.3 21.7 %while.29 = (s32[]{:T(128)}, bf16[2,512,4,64]{1,3,2,0:T(8,128)(2,1)S(1)}, s32[2]{0:T(128)S(1)}, bf16[2,512,4,64]{1,3,2,0:T(8,128)(2,1)S(1)}, f32[2,4,512]{2,1,0:...) while((s32[]{:T(128)}, ...), condition=%wide.region_5.6_spmd.clone.clone, body=%wide.region_0.5_spmd.clone.clone.sunk | while | flops 287052800 | bytes 19649152 | solution.py:59
  58.3 0.6 dynamic_slice.55
  62.2 0.1 broadcast.66
  62.2 4.6 %while.30 = (s32[]{:T(128)}, f32[4,512]{1,0:T(4,128)S(1)}, f32[4,512]{1,0:T(4,128)S(1)}, f32[4,512,64]{1,2,0:T(8,128)S(1)}, s32[]{:T(128)}, /*index=5*/s32[512]{...) while((s32[]{:T(128)}, f32[4,512]{1,0:T(4,128)S(1)}, ...), condition=%wide.region_4.4_spmd, body=%wide.region_1.3_spmd.sunk | while | flops 286790144 | bytes 17768688 | solution.py:55
  62.3 0.2 broadcast_compare_fusion.2
  62.5 1.3 %fusion.33 = (f32[4,512]{1,0:T(4,128)S(1)}, f32[4,512,512]{2,1,0:T(8,128)S(1)}) fusion(f32[4,512]{1,0:T(4,128)S(1)} %dynamic-slice_bitcast_fusion.8, f32[4,512]{1,0:T(4,128)S(1)} %get-tuple-element.413, pred[512,512]{0,1:T(8,128)(4,1)S(1)} %broadcast_compare_fusion.2, bf16[512,4,64]{0,2,1:T(8,128)(2,1)S(1)} %get-tuple-element.412, ...), kind=kOutput, calls=%fused_computation.5.clone.1 | convolution fusion | flops 139458560 | bytes 5005316 | tf_op jit(solution)/shard_map/while/body/eval_jaxpr/while/body/qhe,khe->hqk/dot_general | solution.py:31
  63.8 1.4 %fusion.34 = f32[4,512]{1,0:T(4,128)S(1)} fusion(f32[4,512,512]{2,1,0:T(8,128)S(1)} %get-tuple-element.369, f32[4,512]{1,0:T(4,128)S(1)} %max.4, f32[4,512]{1,0:T(4,128)S(1)} %dynamic-slice_bitcast_fusion.8, f32[4,512]{1,0:T(4,128)S(1)} %get-tuple-element.413, pred[512,512]{0,1:T(8,128)(4,1)S(1)} %broadcast_compare_fusion.2), kind=kLoop, calls=%fused_computation.4.clone.1 | loop fusion | flops 6289408 | bytes 4489216 | tf_op jit(solution)/shard_map/while/body/eval_jaxpr/while/body/reduce_sum | solution.py:41
  65.2 1.6 %fusion.35 = f32[4,512,64]{1,2,0:T(8,128)S(1)} fusion(f32[4,512,512]{2,1,0:T(8,128)S(1)} %get-tuple-element.369, f32[4,512]{1,0:T(4,128)S(1)} %max.4, f32[4,512]{1,0:T(4,128)S(1)} %dynamic-slice_bitcast_fusion.8, f32[4,512]{1,0:T(4,128)S(1)} %get-tuple-element.413, pred[512,512]{0,1:T(8,128)(4,1)S(1)} %broadcast_compare_fusion.2, ...), kind=kOutput, calls=%fused_computation.8.clone.1 | convolution fusion | flops 140771328 | bytes 5799940 | tf_op jit(solution)/shard_map/while/body/eval_jaxpr/while/body/hqk,khe->hqe/dot_general | solution.py:42
  66.9 0.6 dynamic_slice.55
  70.7 0.1 broadcast.66
  70.8 9.1 %while.30 = (s32[]{:T(128)}, f32[4,512]{1,0:T(4,128)S(1)}, f32[4,512]{1,0:T(4,128)S(1)}, f32[4,512,64]{1,2,0:T(8,128)S(1)}, s32[]{:T(128)}, /*index=5*/s32[512]{...) while((s32[]{:T(128)}, f32[4,512]{1,0:T(4,128)S(1)}, ...), condition=%wide.region_4.4_spmd, body=%wide.region_1.3_spmd.sunk | while | flops 286790144 | bytes 17768688 | solution.py:55
  70.9 0.2 broadcast_compare_fusion.2
  71.1 1.3 %fusion.33 = (f32[4,512]{1,0:T(4,128)S(1)}, f32[4,512,512]{2,1,0:T(8,128)S(1)}) fusion(f32[4,512]{1,0:T(4,128)S(1)} %dynamic-slice_bitcast_fusion.8, f32[4,512]{1,0:T(4,128)S(1)} %get-tuple-element.413, pred[512,512]{0,1:T(8,128)(4,1)S(1)} %broadcast_compare_fusion.2, bf16[512,4,64]{0,2,1:T(8,128)(2,1)S(1)} %get-tuple-element.412, ...), kind=kOutput, calls=%fused_computation.5.clone.1 | convolution fusion | flops 139458560 | bytes 5005316 | tf_op jit(solution)/shard_map/while/body/eval_jaxpr/while/body/qhe,khe->hqk/dot_general | solution.py:31
  72.4 1.4 %fusion.34 = f32[4,512]{1,0:T(4,128)S(1)} fusion(f32[4,512,512]{2,1,0:T(8,128)S(1)} %get-tuple-element.369, f32[4,512]{1,0:T(4,128)S(1)} %max.4, f32[4,512]{1,0:T(4,128)S(1)} %dynamic-slice_bitcast_fusion.8, f32[4,512]{1,0:T(4,128)S(1)} %get-tuple-element.413, pred[512,512]{0,1:T(8,128)(4,1)S(1)} %broadcast_compare_fusion.2), kind=kLoop, calls=%fused_computation.4.clone.1 | loop fusion | flops 6289408 | bytes 4489216 | tf_op jit(solution)/shard_map/while/body/eval_jaxpr/while/body/reduce_sum | solution.py:41
  73.8 1.6 %fusion.35 = f32[4,512,64]{1,2,0:T(8,128)S(1)} fusion(f32[4,512,512]{2,1,0:T(8,128)S(1)} %get-tuple-element.369, f32[4,512]{1,0:T(4,128)S(1)} %max.4, f32[4,512]{1,0:T(4,128)S(1)} %dynamic-slice_bitcast_fusion.8, f32[4,512]{1,0:T(4,128)S(1)} %get-tuple-element.413, pred[512,512]{0,1:T(8,128)(4,1)S(1)} %broadcast_compare_fusion.2, ...), kind=kOutput, calls=%fused_computation.8.clone.1 | convolution fusion | flops 140771328 | bytes 5799940 | tf_op jit(solution)/shard_map/while/body/eval_jaxpr/while/body/hqk,khe->hqe/dot_general | solution.py:42
  75.4 0.2 broadcast_compare_fusion.2
  75.7 1.3 %fusion.33 = (f32[4,512]{1,0:T(4,128)S(1)}, f32[4,512,512]{2,1,0:T(8,128)S(1)}) fusion(f32[4,512]{1,0:T(4,128)S(1)} %dynamic-slice_bitcast_fusion.8, f32[4,512]{1,0:T(4,128)S(1)} %get-tuple-element.413, pred[512,512]{0,1:T(8,128)(4,1)S(1)} %broadcast_compare_fusion.2, bf16[512,4,64]{0,2,1:T(8,128)(2,1)S(1)} %get-tuple-element.412, ...), kind=kOutput, calls=%fused_computation.5.clone.1 | convolution fusion | flops 139458560 | bytes 5005316 | tf_op jit(solution)/shard_map/while/body/eval_jaxpr/while/body/qhe,khe->hqk/dot_general | solution.py:31
  77.0 1.4 %fusion.34 = f32[4,512]{1,0:T(4,128)S(1)} fusion(f32[4,512,512]{2,1,0:T(8,128)S(1)} %get-tuple-element.369, f32[4,512]{1,0:T(4,128)S(1)} %max.4, f32[4,512]{1,0:T(4,128)S(1)} %dynamic-slice_bitcast_fusion.8, f32[4,512]{1,0:T(4,128)S(1)} %get-tuple-element.413, pred[512,512]{0,1:T(8,128)(4,1)S(1)} %broadcast_compare_fusion.2), kind=kLoop, calls=%fused_computation.4.clone.1 | loop fusion | flops 6289408 | bytes 4489216 | tf_op jit(solution)/shard_map/while/body/eval_jaxpr/while/body/reduce_sum | solution.py:41
  78.4 1.6 %fusion.35 = f32[4,512,64]{1,2,0:T(8,128)S(1)} fusion(f32[4,512,512]{2,1,0:T(8,128)S(1)} %get-tuple-element.369, f32[4,512]{1,0:T(4,128)S(1)} %max.4, f32[4,512]{1,0:T(4,128)S(1)} %dynamic-slice_bitcast_fusion.8, f32[4,512]{1,0:T(4,128)S(1)} %get-tuple-element.413, pred[512,512]{0,1:T(8,128)(4,1)S(1)} %broadcast_compare_fusion.2, ...), kind=kOutput, calls=%fused_computation.8.clone.1 | convolution fusion | flops 140771328 | bytes 5799940 | tf_op jit(solution)/shard_map/while/body/eval_jaxpr/while/body/hqk,khe->hqe/dot_general | solution.py:42
  80.0 0.7 copy.42
  80.8 0.7 reshape.39
  81.4 3.8 %reduce.3 = bf16[1024,256]{1,0:T(8,128)(2,1)S(1)} reduce(bf16[1024,1,256]{2,1,0:T(2,128)(2,1)S(1)} %bitcast.92, bf16[]{:T(256)} %broadcast.54), dimensions={1}, to_apply=%bitcast.58.reduce_sub_computation | reduce | bytes 1048578
  85.2 0.1 reshape.46
  85.4 13.2 %all_to_all.60 = bf16[4,2,32768]{2,1,0:T(2,128)(2,1)S(1)} all-to-all(bf16[4,2,32768]{2,1,0:T(2,128)(2,1)S(1)} %reshape.46), channel_id=1, replica_groups=mesh['sp'=4,'dp'=8] {'sp'}, dimensions={0} | all-to-all | bytes 1048576 | tf_op jit(solution)/shard_map/all_to_all | solution.py:70
  98.6 0.5 reshape.47
  99.1 0.1 copy.47
  99.2 0.2 copy.40
  99.4 0.0 all-gather.5.cloned.1.call-done
  99.4 4.5 %fusion.20 = bf16[1,256,2112]{1,2,0:T(8,128)(2,1)} fusion(bf16[1024,2112]{0,1:T(8,128)(2,1)} %all-gather.5.cloned.1.call-done, bf16[256,1024]{0,1:T(8,128)(2,1)S(1)} %bitcast.100), kind=kOutput, calls=%fused_computation.29 | convolution fusion | flops 1107836928 | bytes 5931008 | tf_op jit(solution)/shard_map/dot_general | solution.py:77
  (47 shorter events, 0.4 us)
Async XLA Ops:
  6.5 1.0 copy-start
  6.5 13.7 %copy-start.2 = (bf16[1,256,1024]{2,1,0:T(8,128)(2,1)S(1)}, bf16[1,256,1024]{2,1,0:T(8,128)(2,1)}, u32[]{:S(2)}) copy-start(bf16[1,256,1024]{2,1,0:T(8,128)(2,1)} %param.10) | copy-start | bytes 1572868
  6.5 51.7 %all-gather.3.cloned.1.call-start = ((), (), s32[]{:S(2)}) async-start(), calls=%async_computation.4 | async-start | bytes 1216512 | tf_op jit(solution)/shard_map/all_gather | solution.py:75
  15.9 13.1 %all-to-all-start = ((bf16[4,2,32768]{2,1,0:T(2,128)(2,1)}), bf16[4,2,32768]{2,1,0:T(2,128)(2,1)S(1)}, u32[]{:S(2)}, u32[]{:S(2)}) async-start(bf16[4,2,32768]{2,1,0:T(2,128)(2,1)} %reshape.40), calls=%async_computation | async-start | bytes 1048576 | tf_op jit(solution)/shard_map/all_to_all | solution.py:65
  29.0 12.3 %all-to-all-start.1 = ((bf16[4,2,32768]{2,1,0:T(2,128)(2,1)}), bf16[4,2,32768]{2,1,0:T(2,128)(2,1)S(1)}, u32[]{:S(2)}, u32[]{:S(2)}) async-start(bf16[4,2,32768]{2,1,0:T(2,128)(2,1)} %reshape.42), calls=%async_computation.1 | async-start | bytes 1048576 | tf_op jit(solution)/shard_map/all_to_all | solution.py:66
  41.3 13.0 %all-to-all-start.2 = ((bf16[4,2,32768]{2,1,0:T(2,128)(2,1)}), bf16[4,2,32768]{2,1,0:T(2,128)(2,1)}, u32[]{:S(2)}, u32[]{:S(2)}) async-start(bf16[4,2,32768]{2,1,0:T(2,128)(2,1)} %reshape.44), calls=%async_computation.2 | async-start | bytes 1048576 | tf_op jit(solution)/shard_map/all_to_all | solution.py:67
  45.4 54.0 %all-gather.5.cloned.1.call-start = ((), (), s32[]{:S(2)}) async-start(), calls=%async_computation.5 | async-start | bytes 5406720 | tf_op jit(solution)/shard_map/all_gather | solution.py:76
  48.5 9.8 %copy-start.1 = (f32[1,4,1024]{2,1,0:T(4,128)S(1)}, f32[1,4,1024]{2,1,0:T(4,128)}, u32[]{:S(2)}) copy-start(f32[1,4,1024]{2,1,0:T(4,128)} %param.12) | copy-start | bytes 49156
  48.5 9.8 %copy-start.3 = (bf16[2,512,4,64]{1,3,2,0:T(8,128)(2,1)S(1)}, bf16[2,512,4,64]{1,3,2,0:T(8,128)(2,1)}, u32[]{:S(2)}) copy-start(bf16[2,512,4,64]{1,3,2,0:T(8,128)(2,1)} %custom-call) | copy-start | bytes 1572868
  62.5 2.7 %copy-start.4 = (bf16[2,512,4,64]{1,3,2,0:T(8,128)(2,1)S(1)}, bf16[2,512,4,64]{1,3,2,0:T(8,128)(2,1)}, u32[]{:S(2)}) copy-start(bf16[2,512,4,64]{1,3,2,0:T(8,128)(2,1)} %get-tuple-element.415) | copy-start | bytes 1572868 | tf_op jit(solution)/shard_map/while/body/eval_jaxpr/while
  71.1 2.7 %copy-start.4 = (bf16[2,512,4,64]{1,3,2,0:T(8,128)(2,1)S(1)}, bf16[2,512,4,64]{1,3,2,0:T(8,128)(2,1)}, u32[]{:S(2)}) copy-start(bf16[2,512,4,64]{1,3,2,0:T(8,128)(2,1)} %get-tuple-element.415) | copy-start | bytes 1572868 | tf_op jit(solution)/shard_map/while/body/eval_jaxpr/while
  75.7 2.7 %copy-start.4 = (bf16[2,512,4,64]{1,3,2,0:T(8,128)(2,1)S(1)}, bf16[2,512,4,64]{1,3,2,0:T(8,128)(2,1)}, u32[]{:S(2)}) copy-start(bf16[2,512,4,64]{1,3,2,0:T(8,128)(2,1)} %get-tuple-element.415) | copy-start | bytes 1572868 | tf_op jit(solution)/shard_map/while/body/eval_jaxpr/while
Sparse Core Ops, SparseCore 0:
  9.5 43.1 all-gather.2
  58.4 38.7 all-gather.4
where the time goes:
time: 111 us
  local copies, waits for them, and re-layouts  21.2 us (19%)
  other arithmetic  20.1 us (18%)
  between operations  13.7 us (12%)
  blocking collectives  13.2 us (12%)
  matrix products  13 us (12%)
  starting transfers between devices  12.1 us (11%)
  waiting for transfers between devices  10.6 us (10%)
  loops' own time  6.82 us (6%)
    unnamed x27, local copies, waits for them, and re-layouts  15.2 us
    unnamed x4, other arithmetic  15.2 us
    all_to_all x1, blocking collectives, body(): lax.all_to_all(local_out[None], 'sp', split_axis=1, concat_axis=2, tiled=...  13.2 us
    another operation x1, loops' own time, attend(): outputs = lax.map(one_block, jnp.arange(block_count, dtype=jnp.int32))  6.51 us
    all_to_all x1, waiting for transfers between devices, body(): lax.all_to_all(values, 'sp', split_axis=2, concat_axis=1, tiled=True)  5.69 us
    dot_general x3, matrix products, key_step(): jnp.einsum('hqk,khe->hqe', scores.astype(jnp.bfloat16), value_part, prefe...  4.72 us
    dot_general x1, matrix products, body(): mixed = jnp.dot(attended, whole_weight, preferred_element_type=jnp.float32)  4.5 us
    all_to_all x1, starting transfers between devices, body(): lax.all_to_all(queries, 'sp', split_axis=2, concat_axis=1, tiled=True)  4.26 us
  transfers between devices with their start and end apart: 5, of which 3 were waited for; matrix products, arithmetic and copies ran while one was open for 43% of the time, Pallas kernels for 0%

commit v1 on v0

--- a/solution.py
+++ b/solution.py
@@ -64,7 +64,10 @@
     query_heads, key_heads, value_heads = (
         lax.all_to_all(queries, "sp", split_axis=2, concat_axis=1, tiled=True),
         lax.all_to_all(keys, "sp", split_axis=2, concat_axis=1, tiled=True),
-        lax.all_to_all(values, "sp", split_axis=2, concat_axis=1, tiled=True),
+        jnp.concatenate(
+            lax.all_to_all(jnp.stack(jnp.split(values, lax.axis_size("sp"), axis=2)), "sp", 0, 0),
+            axis=1,
+        ),
     )
     local_out = attend(query_heads[0], key_heads[0], value_heads[0], cum_gate[0])
     attended = lax.all_to_all(local_out[None], "sp", split_axis=1, concat_axis=2, tiled=True)[0]

time: 111 us -> 106 us (0.955)
  local copies, waits for them, and re-layouts: 21.2 us -> 17.8 us
  waiting for transfers between devices: 10.6 us -> 13.1 us
  blocking collectives: 13.2 us -> 11.3 us
  other arithmetic: 20.1 us -> 18.6 us
    unnamed x27 -> x21, local copies, waits for them, and re-layouts: 15.2 us -> 10.1 us
    all_to_all x1, waiting for transfers between devices: 5.69 us -> 1.14 us  [body(): lax.all_to_all(jnp.stack(jnp.split(values, lax.axis_size('sp'), axis=2)),...]
    unnamed x4 -> x3, other arithmetic: 15.2 us -> 11.4 us
    all_to_all x1, waiting for transfers between devices: 1.66 us -> 5.33 us  [body(): lax.all_to_all(keys, 'sp', split_axis=2, concat_axis=1, tiled=True)]
    all_gather x1, waiting for transfers between devices: 0.01 us -> 3.39 us  [body(): full_rows = lax.all_gather(own_rows, 'dp', axis=1, tiled=True)]
    all_to_all x1, blocking collectives: 13.2 us -> 11.3 us  [body(): lax.all_to_all(local_out[None], 'sp', split_axis=1, concat_axis=2, tiled=...]
    dynamic_update_slice x2, other arithmetic: 0.1 us -> 1.51 us  [attend(): outputs = lax.map(one_block, jnp.arange(block_count, dtype=jnp.int32))]
    another operation x6 -> x7, local copies, waits for them, and re-layouts: 0.11 us -> 1.31 us  [the longest x1 1.2 us: body(): jnp.stack(jnp.split(values, lax.axis_size('sp'), axis=2))]
  transfers between devices with their start and end apart: 5 -> 5, of which waited for: 3 -> 4; matrix products, arithmetic and copies ran while one was open for 43% -> 41% of each run, Pallas kernels for 0% -> 0%
where the time goes in v1:
time: 106 us
  other arithmetic  18.6 us (18%)
  local copies, waits for them, and re-layouts  17.8 us (17%)
  between operations  13.6 us (13%)
  waiting for transfers between devices  13.1 us (12%)
  matrix products  13 us (12%)
  starting transfers between devices  11.4 us (11%)
  blocking collectives  11.3 us (11%)
  loops' own time  6.76 us (6%)
    unnamed x3, other arithmetic  11.4 us
    all_to_all x1, blocking collectives, body(): lax.all_to_all(local_out[None], 'sp', split_axis=1, concat_axis=2, tiled=...  11.3 us
    unnamed x21, local copies, waits for them, and re-layouts  10.1 us
    another operation x1, loops' own time, attend(): outputs = lax.map(one_block, jnp.arange(block_count, dtype=jnp.int32))  6.45 us
    all_to_all x1, waiting for transfers between devices, body(): lax.all_to_all(keys, 'sp', split_axis=2, concat_axis=1, tiled=True)  5.33 us
    dot_general x3, matrix products, key_step(): jnp.einsum('hqk,khe->hqe', scores.astype(jnp.bfloat16), value_part, prefe...  4.7 us
    dot_general x1, matrix products, body(): mixed = jnp.dot(attended, whole_weight, preferred_element_type=jnp.float32)  4.5 us
    all_to_all x1, starting transfers between devices, body(): lax.all_to_all(jnp.stack(jnp.split(values, lax.axis_size('sp'), axis=2)),...  4.26 us
  transfers between devices with their start and end apart: 5, of which 4 were waited for; matrix products, arithmetic and copies ran while one was open for 41% of the time, Pallas kernels for 0%

profile of v1, /device:TPU:0, one launch (start us, length us, event | category | flops | bytes accessed | tf_op | source)
XLA Modules:
  0.0 105.7 jit_solution(14559300406368657453)
XLA Ops:
  6.5 1.0 copy-done
  7.6 0.7 constant_dynamic-slice_fusion
  8.2 0.0 all-gather.3.cloned.1.call-update
  8.3 1.2 %slice_bitcast_fusion.3 = (bf16[1,1,256,256]{3,2,1,0:T(8,128)(2,1)S(1)}, bf16[1,1,256,256]{3,2,1,0:T(8,128)(2,1)S(1)}, bf16[1,1,256,256]{3,2,1,0:T(8,128)(2,1)S(1)}, bf16[1,1,256,256]{3,2,1,0:T(8,128)(2,1)S(1)}) fusion(bf16[1,256,1024]{2,1,0:T(8,128)(2,1)} %param.11), kind=kLoop, calls=%fused_computation.34 | loop fusion | bytes 1048576 | tf_op jit(solution)/shard_map/stack | solution.py:68
  9.5 0.9 pad_maximum_fusion
  10.3 4.3 %all-to-all-start.2 = ((bf16[4,1,256,256]{3,2,1,0:T(8,128)(2,1)}), bf16[4,1,256,256]{3,2,1,0:T(8,128)(2,1)S(1)}, u32[]{:S(2)}, u32[]{:S(2)}) async-start(bf16[4,1,256,256]{3,2,1,0:T(8,128)(2,1)} %pad_maximum_fusion), calls=%async_computation.2 | async-start | bytes 1048576 | tf_op jit(solution)/shard_map/all_to_all | solution.py:68
  14.6 2.4 %copy.28 = bf16[1,256,1024]{1,0,2:T(2,128)(2,1)S(1)} copy(bf16[1,256,1024]{2,1,0:T(8,128)(2,1)} %param.9) | data formatting | bytes 1048576 | tf_op args[0]
  17.0 0.5 broadcast.54
  17.6 3.8 %reduce = bf16[1024,256]{1,0:T(8,128)(2,1)S(1)} reduce(bf16[1024,1,256]{2,1,0:T(2,128)(2,1)S(1)} %bitcast.93, bf16[]{:T(256)} %broadcast.54), dimensions={1}, to_apply=%bitcast.57.reduce_sub_computation | reduce | bytes 1048578
  21.4 0.9 reshape.40
  22.3 1.1 %all-to-all-done.2 = bf16[4,1,256,256]{3,2,1,0:T(8,128)(2,1)S(1)} async-done(((bf16[4,1,256,256]{3,2,1,0:T(8,128)(2,1)}), bf16[4,1,256,256]{3,2,1,0:T(8,128)(2,1)S(1)}, u32[]{:S(2)}, u32[]{:S(2)}) %all-to-all-start.2) | async-done | bytes 524320 | tf_op jit(solution)/shard_map/all_to_all | solution.py:68
  23.4 3.5 %all-to-all-start = ((bf16[4,2,32768]{2,1,0:T(2,128)(2,1)}), bf16[4,2,32768]{2,1,0:T(2,128)(2,1)S(1)}, u32[]{:S(2)}, u32[]{:S(2)}) async-start(bf16[4,2,32768]{2,1,0:T(2,128)(2,1)} %reshape.40), calls=%async_computation | async-start | bytes 1048576 | tf_op jit(solution)/shard_map/all_to_all | solution.py:65
  26.9 0.9 copy.30
  27.8 3.8 %reduce.1 = bf16[1024,256]{1,0:T(8,128)(2,1)S(1)} reduce(bf16[1024,1,256]{2,1,0:T(2,128)(2,1)S(1)} %bitcast.95, bf16[]{:T(256)} %broadcast.54), dimensions={1}, to_apply=%bitcast.59.reduce_sub_computation | reduce | bytes 1048578
  31.6 0.9 reshape.42
  32.5 3.2 %all-to-all-done = bf16[4,2,32768]{2,1,0:T(2,128)(2,1)S(1)} async-done(((bf16[4,2,32768]{2,1,0:T(2,128)(2,1)}), bf16[4,2,32768]{2,1,0:T(2,128)(2,1)S(1)}, u32[]{:S(2)}, u32[]{:S(2)}) %all-to-all-start) | async-done | bytes 524320 | tf_op jit(solution)/shard_map/all_to_all | solution.py:65
  35.7 3.5 %all-to-all-start.1 = ((bf16[4,2,32768]{2,1,0:T(2,128)(2,1)}), bf16[4,2,32768]{2,1,0:T(2,128)(2,1)S(1)}, u32[]{:S(2)}, u32[]{:S(2)}) async-start(bf16[4,2,32768]{2,1,0:T(2,128)(2,1)} %reshape.42), calls=%async_computation.1 | async-start | bytes 1048576 | tf_op jit(solution)/shard_map/all_to_all | solution.py:66
  39.2 0.2 all-gather.5.cloned.1.call-start
  39.4 0.4 reshape.38
  39.8 1.4 %copy.35 = bf16[2,512,4,64]{1,3,2,0:T(8,128)(2,1)} copy(bf16[2,512,4,64]{3,2,1,0:T(4,128)(2,1)S(1)} %reshape.38) | data formatting | bytes 1048576
  41.2 0.5 reshape.41
  41.7 0.1 copy.44
  41.8 0.4 copy.29
  42.2 0.3 reshape_squeeze.9
  42.5 0.1 copy.33
  42.6 5.3 %all-to-all-done.1 = bf16[4,2,32768]{2,1,0:T(2,128)(2,1)S(1)} async-done(((bf16[4,2,32768]{2,1,0:T(2,128)(2,1)}), bf16[4,2,32768]{2,1,0:T(2,128)(2,1)S(1)}, u32[]{:S(2)}, u32[]{:S(2)}) %all-to-all-start.1) | async-done | bytes 524320 | tf_op jit(solution)/shard_map/all_to_all | solution.py:66
  47.9 0.5 reshape.43
  48.5 0.1 copy.45
  48.6 0.4 copy.31
  49.0 0.3 reshape_squeeze.11
  49.3 0.1 copy.34
  49.4 3.4 %all-gather.3.cloned.1.call-done = bf16[256,2112]{0,1:T(8,128)(2,1)} async-done(((bf16[256,264]{0,1:T(8,128)(2,1)}), bf16[256,2112]{0,1:T(8,128)(2,1)}) %all-gather.3.cloned.1.call-update) | async-done | bytes 1081360 | tf_op jit(solution)/shard_map/all_gather | solution.py:78
  52.8 0.0 all-gather.5.cloned.1.call-update
  52.8 23.0 %while.29 = (s32[]{:T(128)}, bf16[2,512,4,64]{1,3,2,0:T(8,128)(2,1)}, s32[2]{0:T(128)S(1)}, bf16[2,512,4,64]{1,3,2,0:T(8,128)(2,1)S(1)}, f32[2,4,512]{2,1,0:T(4,...) while((s32[]{:T(128)}, ...), condition=%wide.region_5.6_spmd.clone.clone, body=%wide.region_0.5_spmd.clone.clone.sunk | while | flops 287052800 | bytes 19649660 | solution.py:59
  52.8 0.6 dynamic_slice.55
  56.7 0.1 broadcast.65
  56.8 4.6 %while.30 = (s32[]{:T(128)}, f32[4,512]{1,0:T(4,128)S(1)}, f32[4,512]{1,0:T(4,128)S(1)}, f32[4,512,64]{1,2,0:T(8,128)S(1)}, s32[]{:T(128)}, /*index=5*/s32[512]{...) while((s32[]{:T(128)}, f32[4,512]{1,0:T(4,128)S(1)}, ...), condition=%wide.region_4.4_spmd, body=%wide.region_1.3_spmd.sunk | while | flops 286790144 | bytes 17768688 | solution.py:55
  56.8 0.2 broadcast_compare_fusion.2
  57.0 1.3 %fusion.33 = (f32[4,512]{1,0:T(4,128)S(1)}, f32[4,512,512]{2,1,0:T(8,128)S(1)}) fusion(f32[4,512]{1,0:T(4,128)S(1)} %dynamic-slice_bitcast_fusion.8, f32[4,512]{1,0:T(4,128)S(1)} %get-tuple-element.417, pred[512,512]{0,1:T(8,128)(4,1)S(1)} %broadcast_compare_fusion.2, bf16[512,4,64]{0,2,1:T(8,128)(2,1)S(1)} %get-tuple-element.416, ...), kind=kOutput, calls=%fused_computation.5.clone.1 | convolution fusion | flops 139458560 | bytes 5005316 | tf_op jit(solution)/shard_map/while/body/eval_jaxpr/while/body/qhe,khe->hqk/dot_general | solution.py:31
  58.3 1.4 %fusion.34 = f32[4,512]{1,0:T(4,128)S(1)} fusion(f32[4,512,512]{2,1,0:T(8,128)S(1)} %get-tuple-element.373, f32[4,512]{1,0:T(4,128)S(1)} %max.4, f32[4,512]{1,0:T(4,128)S(1)} %dynamic-slice_bitcast_fusion.8, f32[4,512]{1,0:T(4,128)S(1)} %get-tuple-element.417, pred[512,512]{0,1:T(8,128)(4,1)S(1)} %broadcast_compare_fusion.2), kind=kLoop, calls=%fused_computation.4.clone.1 | loop fusion | flops 6289408 | bytes 4489216 | tf_op jit(solution)/shard_map/while/body/eval_jaxpr/while/body/reduce_sum | solution.py:41
  59.7 1.6 %fusion.35 = f32[4,512,64]{1,2,0:T(8,128)S(1)} fusion(f32[4,512,512]{2,1,0:T(8,128)S(1)} %get-tuple-element.373, f32[4,512]{1,0:T(4,128)S(1)} %max.4, f32[4,512]{1,0:T(4,128)S(1)} %dynamic-slice_bitcast_fusion.8, f32[4,512]{1,0:T(4,128)S(1)} %get-tuple-element.417, pred[512,512]{0,1:T(8,128)(4,1)S(1)} %broadcast_compare_fusion.2, ...), kind=kOutput, calls=%fused_computation.8.clone.1 | convolution fusion | flops 140771328 | bytes 5799940 | tf_op jit(solution)/shard_map/while/body/eval_jaxpr/while/body/hqk,khe->hqe/dot_general | solution.py:42
  61.3 0.8 bitcast_dynamic-update-slice_fusion.2
  62.1 0.6 dynamic_slice.55
  65.9 0.1 broadcast.65
  66.0 9.1 %while.30 = (s32[]{:T(128)}, f32[4,512]{1,0:T(4,128)S(1)}, f32[4,512]{1,0:T(4,128)S(1)}, f32[4,512,64]{1,2,0:T(8,128)S(1)}, s32[]{:T(128)}, /*index=5*/s32[512]{...) while((s32[]{:T(128)}, f32[4,512]{1,0:T(4,128)S(1)}, ...), condition=%wide.region_4.4_spmd, body=%wide.region_1.3_spmd.sunk | while | flops 286790144 | bytes 17768688 | solution.py:55
  66.1 0.2 broadcast_compare_fusion.2
  66.3 1.3 %fusion.33 = (f32[4,512]{1,0:T(4,128)S(1)}, f32[4,512,512]{2,1,0:T(8,128)S(1)}) fusion(f32[4,512]{1,0:T(4,128)S(1)} %dynamic-slice_bitcast_fusion.8, f32[4,512]{1,0:T(4,128)S(1)} %get-tuple-element.417, pred[512,512]{0,1:T(8,128)(4,1)S(1)} %broadcast_compare_fusion.2, bf16[512,4,64]{0,2,1:T(8,128)(2,1)S(1)} %get-tuple-element.416, ...), kind=kOutput, calls=%fused_computation.5.clone.1 | convolution fusion | flops 139458560 | bytes 5005316 | tf_op jit(solution)/shard_map/while/body/eval_jaxpr/while/body/qhe,khe->hqk/dot_general | solution.py:31
  67.6 1.4 %fusion.34 = f32[4,512]{1,0:T(4,128)S(1)} fusion(f32[4,512,512]{2,1,0:T(8,128)S(1)} %get-tuple-element.373, f32[4,512]{1,0:T(4,128)S(1)} %max.4, f32[4,512]{1,0:T(4,128)S(1)} %dynamic-slice_bitcast_fusion.8, f32[4,512]{1,0:T(4,128)S(1)} %get-tuple-element.417, pred[512,512]{0,1:T(8,128)(4,1)S(1)} %broadcast_compare_fusion.2), kind=kLoop, calls=%fused_computation.4.clone.1 | loop fusion | flops 6289408 | bytes 4489216 | tf_op jit(solution)/shard_map/while/body/eval_jaxpr/while/body/reduce_sum | solution.py:41
  69.0 1.6 %fusion.35 = f32[4,512,64]{1,2,0:T(8,128)S(1)} fusion(f32[4,512,512]{2,1,0:T(8,128)S(1)} %get-tuple-element.373, f32[4,512]{1,0:T(4,128)S(1)} %max.4, f32[4,512]{1,0:T(4,128)S(1)} %dynamic-slice_bitcast_fusion.8, f32[4,512]{1,0:T(4,128)S(1)} %get-tuple-element.417, pred[512,512]{0,1:T(8,128)(4,1)S(1)} %broadcast_compare_fusion.2, ...), kind=kOutput, calls=%fused_computation.8.clone.1 | convolution fusion | flops 140771328 | bytes 5799940 | tf_op jit(solution)/shard_map/while/body/eval_jaxpr/while/body/hqk,khe->hqe/dot_general | solution.py:42
  70.6 0.2 broadcast_compare_fusion.2
  70.8 1.3 %fusion.33 = (f32[4,512]{1,0:T(4,128)S(1)}, f32[4,512,512]{2,1,0:T(8,128)S(1)}) fusion(f32[4,512]{1,0:T(4,128)S(1)} %dynamic-slice_bitcast_fusion.8, f32[4,512]{1,0:T(4,128)S(1)} %get-tuple-element.417, pred[512,512]{0,1:T(8,128)(4,1)S(1)} %broadcast_compare_fusion.2, bf16[512,4,64]{0,2,1:T(8,128)(2,1)S(1)} %get-tuple-element.416, ...), kind=kOutput, calls=%fused_computation.5.clone.1 | convolution fusion | flops 139458560 | bytes 5005316 | tf_op jit(solution)/shard_map/while/body/eval_jaxpr/while/body/qhe,khe->hqk/dot_general | solution.py:31
  72.1 1.4 %fusion.34 = f32[4,512]{1,0:T(4,128)S(1)} fusion(f32[4,512,512]{2,1,0:T(8,128)S(1)} %get-tuple-element.373, f32[4,512]{1,0:T(4,128)S(1)} %max.4, f32[4,512]{1,0:T(4,128)S(1)} %dynamic-slice_bitcast_fusion.8, f32[4,512]{1,0:T(4,128)S(1)} %get-tuple-element.417, pred[512,512]{0,1:T(8,128)(4,1)S(1)} %broadcast_compare_fusion.2), kind=kLoop, calls=%fused_computation.4.clone.1 | loop fusion | flops 6289408 | bytes 4489216 | tf_op jit(solution)/shard_map/while/body/eval_jaxpr/while/body/reduce_sum | solution.py:41
  73.5 1.6 %fusion.35 = f32[4,512,64]{1,2,0:T(8,128)S(1)} fusion(f32[4,512,512]{2,1,0:T(8,128)S(1)} %get-tuple-element.373, f32[4,512]{1,0:T(4,128)S(1)} %max.4, f32[4,512]{1,0:T(4,128)S(1)} %dynamic-slice_bitcast_fusion.8, f32[4,512]{1,0:T(4,128)S(1)} %get-tuple-element.417, pred[512,512]{0,1:T(8,128)(4,1)S(1)} %broadcast_compare_fusion.2, ...), kind=kOutput, calls=%fused_computation.8.clone.1 | convolution fusion | flops 140771328 | bytes 5799940 | tf_op jit(solution)/shard_map/while/body/eval_jaxpr/while/body/hqk,khe->hqe/dot_general | solution.py:42
  75.1 0.8 bitcast_dynamic-update-slice_fusion.2
  75.9 1.6 %copy.42 = bf16[2,512,4,64]{3,2,1,0:T(4,128)(2,1)S(1)} copy(bf16[2,512,4,64]{1,3,2,0:T(8,128)(2,1)} %get-tuple-element.478) | data formatting | bytes 1048576 | tf_op jit(solution)/shard_map/broadcast_in_dim;reshape | solution.py:73
  77.5 0.7 reshape.39
  78.2 3.8 %reduce.2 = bf16[1024,256]{1,0:T(8,128)(2,1)S(1)} reduce(bf16[1024,1,256]{2,1,0:T(2,128)(2,1)S(1)} %bitcast.94, bf16[]{:T(256)} %broadcast.54), dimensions={1}, to_apply=%bitcast.61.reduce_sub_computation | reduce | bytes 1048578
  82.0 0.1 reshape.44
  82.1 11.3 %all_to_all.50 = bf16[4,2,32768]{2,1,0:T(2,128)(2,1)S(1)} all-to-all(bf16[4,2,32768]{2,1,0:T(2,128)(2,1)S(1)} %reshape.44), channel_id=1, replica_groups=mesh['sp'=4,'dp'=8] {'sp'}, dimensions={0} | all-to-all | bytes 1048576 | tf_op jit(solution)/shard_map/all_to_all | solution.py:73
  93.5 0.5 reshape.45
  94.0 0.1 copy.46
  94.1 0.2 copy.38
  94.3 0.0 all-gather.5.cloned.1.call-done
  94.3 4.5 %fusion.20 = bf16[1,256,2112]{1,2,0:T(8,128)(2,1)} fusion(bf16[1024,2112]{0,1:T(8,128)(2,1)} %all-gather.5.cloned.1.call-done, bf16[256,1024]{0,1:T(8,128)(2,1)S(1)} %bitcast.100), kind=kOutput, calls=%fused_computation.29 | convolution fusion | flops 1107836928 | bytes 5931008 | tf_op jit(solution)/shard_map/dot_general | solution.py:80
  (41 shorter events, 0.2 us)
Async XLA Ops:
  6.5 1.0 copy-start
  6.5 46.2 %all-gather.3.cloned.1.call-start = ((), (), s32[]{:S(2)}) async-start(), calls=%async_computation.4 | async-start | bytes 1216512 | tf_op jit(solution)/shard_map/all_gather | solution.py:78
  8.3 18.6 %copy-start.2 = (bf16[1,256,1024]{2,1,0:T(8,128)(2,1)S(1)}, bf16[1,256,1024]{2,1,0:T(8,128)(2,1)}, u32[]{:S(2)}) copy-start(bf16[1,256,1024]{2,1,0:T(8,128)(2,1)} %param.10) | copy-start | bytes 1572868
  10.3 13.1 %all-to-all-start.2 = ((bf16[4,1,256,256]{3,2,1,0:T(8,128)(2,1)}), bf16[4,1,256,256]{3,2,1,0:T(8,128)(2,1)S(1)}, u32[]{:S(2)}, u32[]{:S(2)}) async-start(bf16[4,1,256,256]{3,2,1,0:T(8,128)(2,1)} %pad_maximum_fusion), calls=%async_computation.2 | async-start | bytes 1048576 | tf_op jit(solution)/shard_map/all_to_all | solution.py:68
  23.4 12.3 %all-to-all-start = ((bf16[4,2,32768]{2,1,0:T(2,128)(2,1)}), bf16[4,2,32768]{2,1,0:T(2,128)(2,1)S(1)}, u32[]{:S(2)}, u32[]{:S(2)}) async-start(bf16[4,2,32768]{2,1,0:T(2,128)(2,1)} %reshape.40), calls=%async_computation | async-start | bytes 1048576 | tf_op jit(solution)/shard_map/all_to_all | solution.py:65
  35.7 12.3 %all-to-all-start.1 = ((bf16[4,2,32768]{2,1,0:T(2,128)(2,1)}), bf16[4,2,32768]{2,1,0:T(2,128)(2,1)S(1)}, u32[]{:S(2)}, u32[]{:S(2)}) async-start(bf16[4,2,32768]{2,1,0:T(2,128)(2,1)} %reshape.42), calls=%async_computation.1 | async-start | bytes 1048576 | tf_op jit(solution)/shard_map/all_to_all | solution.py:66
  39.2 55.1 %all-gather.5.cloned.1.call-start = ((), (), s32[]{:S(2)}) async-start(), calls=%async_computation.5 | async-start | bytes 5406720 | tf_op jit(solution)/shard_map/all_gather | solution.py:79
  42.5 10.3 %copy-start.1 = (f32[1,4,1024]{2,1,0:T(4,128)S(1)}, f32[1,4,1024]{2,1,0:T(4,128)}, u32[]{:S(2)}) copy-start(f32[1,4,1024]{2,1,0:T(4,128)} %param.12) | copy-start | bytes 49156
  57.0 2.7 %copy-start.3 = (bf16[2,512,4,64]{1,3,2,0:T(8,128)(2,1)S(1)}, bf16[2,512,4,64]{1,3,2,0:T(8,128)(2,1)}, u32[]{:S(2)}) copy-start(bf16[2,512,4,64]{1,3,2,0:T(8,128)(2,1)} %get-tuple-element.419) | copy-start | bytes 1572868 | tf_op jit(solution)/shard_map/while/body/eval_jaxpr/while
  66.3 2.7 %copy-start.3 = (bf16[2,512,4,64]{1,3,2,0:T(8,128)(2,1)S(1)}, bf16[2,512,4,64]{1,3,2,0:T(8,128)(2,1)}, u32[]{:S(2)}) copy-start(bf16[2,512,4,64]{1,3,2,0:T(8,128)(2,1)} %get-tuple-element.419) | copy-start | bytes 1572868 | tf_op jit(solution)/shard_map/while/body/eval_jaxpr/while
  70.8 2.7 %copy-start.3 = (bf16[2,512,4,64]{1,3,2,0:T(8,128)(2,1)S(1)}, bf16[2,512,4,64]{1,3,2,0:T(8,128)(2,1)}, u32[]{:S(2)}) copy-start(bf16[2,512,4,64]{1,3,2,0:T(8,128)(2,1)} %get-tuple-element.419) | copy-start | bytes 1572868 | tf_op jit(solution)/shard_map/while/body/eval_jaxpr/while
Sparse Core Ops, SparseCore 0:
  9.5 43.2 all-gather.2
  54.3 34.4 all-gather.4
